TPU v7x, 32 devices: a whole 2x2x4 slice. The times are simulated.
32 devices in a mesh: sp: 16 (over z, y, x), tp: 2 (over core).
Axes of the slice: x: 2, y: 2, z: 4, core: 2. Of those that a mesh axis runs over, the one named last changes fastest.
Arguments:
- tokens: bfloat16 [4096, 4096], P('sp'), may hold values from -5 to 5
- documents: int32 [4096], P('sp'), may hold values from 0 to 3, never falling along the last dimension, each value on 1 to 2048 neighbouring positions
- norm_gain: float32 [2, 4096], replicated, may hold values from 0.1 to 1.9
- in_weight: bfloat16 [2, 4096, 2048], P(None, 'sp', 'tp'), may hold values from -0.09375 to 0.09375
- conv_taps: float32 [2, 4, 2048], P(None, None, 'tp'), may hold values from -3 to 3
- conv_bias: float32 [2, 2048], P(None, 'tp'), may hold values from -0.75 to 0.75
- recur_gate: bfloat16 [2, 32, 64, 64], P(None, 'tp'), may hold values from -0.75 to 0.75
- input_gate: bfloat16 [2, 32, 64, 64], P(None, 'tp'), may hold values from -0.75 to 0.75
- recur_bias: float32 [2, 2048], P(None, 'tp'), may hold values from -4 to 4
- input_bias: float32 [2, 2048], P(None, 'tp'), may hold values from -4 to 4
- decay_param: float32 [2, 2048], P(None, 'tp'), may hold values from 4 to 7
- out_weight: bfloat16 [2, 2048, 4096], P(None, 'tp', 'sp'), may hold values from -0.375 to 0.375
Outputs:
- layered: bfloat16 [4096, 4096], P('sp')
All inputs are finite; a program needn't handle non-finite values.
Results may differ from a plain program's by a relative error of at most 0.017.
Values may be sent and summed in bfloat16 or wider, within the bound.
No kernel may reach another device: no remote copies, remote signals or barrier semaphores. Data moves between devices by JAX's collectives and lax.ppermute only.
A program may use at most 128 MiB of HBM per device.

v0:
```python
import jax
import jax.numpy as jnp
from jax import lax
from jax.sharding import PartitionSpec as P

RG_C = 8.0
EPS = 0.1


def passed_along(block, axis, distance):
    devices = range(lax.axis_size(axis))
    route = [(i - distance, i) for i in devices if i - distance in devices]
    return lax.ppermute(block, axis, route)


def carried_in(part, axis, combine, identity):
    place = lax.axis_index(axis)
    gathered = jax.tree.map(lambda a: lax.all_gather(a, axis), part)
    state = jax.tree.map(lambda a, e: jnp.zeros_like(a) + jnp.asarray(e, a.dtype), part, identity)

    def one(hop, state):
        return combine(
            state, jax.tree.map(lambda a: lax.dynamic_index_in_dim(a, hop, 0, False), gathered)
        )

    return lax.fori_loop(0, place, one, state)


def norm_rows(values_in, gain_row):
    values = values_in.astype(jnp.float32)
    scaled = values * lax.rsqrt(jnp.mean(values * values, axis=-1, keepdims=True) + EPS)
    return (scaled * gain_row[None, :]).astype(jnp.bfloat16)


def combine(earlier, following):
    return (earlier[0] * following[0], following[0] * earlier[1] + following[1])


def per_device(
    tokens,
    documents,
    norm_gain,
    in_weight,
    conv_taps,
    conv_bias,
    recur_gate,
    input_gate,
    recur_bias,
    input_bias,
    decay_param,
    out_weight,
):
    num_rows = tokens.shape[0]
    layer_count = in_weight.shape[0]
    chan_width = in_weight.shape[2]
    tap_count = conv_taps.shape[1]
    blocks = recur_gate.shape[1]
    block_dim = recur_gate.shape[2]
    doc_values = documents.astype(jnp.bfloat16)
    whole_in, whole_out = (
        lax.all_gather(in_weight, "sp", axis=1, tiled=True),
        lax.all_gather(out_weight, "sp", axis=2, tiled=True),
    )
    state_x = tokens
    for depth_at in range(layer_count):
        normed = norm_rows(state_x, norm_gain[depth_at])
        projected = jnp.dot(normed, whole_in[depth_at], preferred_element_type=jnp.float32)
        mixed_in = projected.astype(jnp.bfloat16)
        cut_at = num_rows - tap_count + 1
        tail_in, tail_doc = passed_along((mixed_in[cut_at:], doc_values[cut_at:]), "sp", 1)
        ext_in = jnp.concatenate([tail_in, mixed_in], axis=0).astype(jnp.float32)
        ext_doc = jnp.concatenate([tail_doc, doc_values], axis=0)
        first = tap_count - 1
        conv_sum = conv_bias[depth_at][None, :] + conv_taps[depth_at, 0][None, :] * ext_in[first:]
        for lag_step in range(1, tap_count):
            low = first - lag_step
            same_doc = (ext_doc[low : low + num_rows] == doc_values)[:, None]
            conv_sum = conv_sum + jnp.where(
                same_doc, conv_taps[depth_at, lag_step][None, :] * ext_in[low : low + num_rows], 0.0
            )
        conv_out = conv_sum.astype(jnp.bfloat16)
        grouped = conv_out.reshape(num_rows, blocks, block_dim)
        recur_rate = jax.nn.sigmoid(
            jnp.einsum(
                "snb,nbc->snc", grouped, recur_gate[depth_at], preferred_element_type=jnp.float32
            ).reshape(num_rows, chan_width)
            + recur_bias[depth_at][None, :]
        )
        input_rate = jax.nn.sigmoid(
            jnp.einsum(
                "snb,nbc->snc", grouped, input_gate[depth_at], preferred_element_type=jnp.float32
            ).reshape(num_rows, chan_width)
            + input_bias[depth_at][None, :]
        )
        reset = ext_doc[first - 1 : first - 1 + num_rows] != doc_values
        log_decay = -RG_C * jax.nn.softplus(-decay_param[depth_at])[None, :] * recur_rate
        decay_now = jnp.where(reset[:, None], 0.0, jnp.exp(log_decay))
        drive_term = jnp.sqrt(jnp.maximum(-jnp.expm1(2.0 * log_decay), 0.0)) * (
            input_rate * conv_out.astype(jnp.float32)
        )
        cum_decay, local_state = lax.associative_scan(combine, (decay_now, drive_term), axis=0)
        identity = (jnp.ones((chan_width,), jnp.float32), jnp.zeros((chan_width,), jnp.float32))
        _, carried = carried_in(
            (cum_decay[num_rows - 1], local_state[num_rows - 1]), "sp", combine, identity
        )
        hidden = (local_state + cum_decay * carried[None, :]).astype(jnp.bfloat16)
        partial_sum = jnp.dot(hidden, whole_out[depth_at], preferred_element_type=jnp.float32)
        summed = lax.psum(partial_sum.astype(jnp.bfloat16), "tp").astype(jnp.float32)
        state_x = (state_x.astype(jnp.float32) + summed).astype(jnp.bfloat16)
    return state_x


def solution(mesh):
    return jax.shard_map(
        per_device,
        mesh=mesh,
        in_specs=(
            P("sp", None),
            P("sp"),
            P(),
            P(None, "sp", "tp"),
            P(None, None, "tp"),
            P(None, "tp"),
            P(None, "tp", None, None),
            P(None, "tp", None, None),
            P(None, "tp"),
            P(None, "tp"),
            P(None, "tp"),
            P(None, "tp", "sp"),
        ),
        out_specs=P("sp", None),
        check_vma=False,
    )
```

profile of v0, /device:TPU:0, one launch (start us, length us, event | category | flops | bytes accessed | tf_op | source)
XLA Modules:
  0.0 754.7 jit_solution(14435381683469304299)
XLA Ops:
  8.9 4.9 collective-permute-start.1
  19.6 184.4 %all-gather.7.cloned.1.call-done = bf16[2,4096,1024]{2,1,0:T(8,128)(2,1)} async-done(((bf16[2,256,1024]{2,1,0:T(8,128)(2,1)}), bf16[2,4096,1024]{2,1,0:T(8,128)(2,1)}) %all-gather.7.cloned.1.call-update) | async-done | bytes 16777232 | tf_op jit(solution)/shard_map/all_gather | solution.py:61
  204.0 5.8 fusion.20
  227.7 4.2 multiply_multiply_fusion.1
  310.2 3.3 slice.677
  330.4 4.7 pad.211
  349.3 41.5 %all-gather.1 = f32[16,1,1024]{2,1,0:T(1,128)S(1)} all-gather(f32[1,1,1024]{2,1,0:T(1,128)S(1)} %add_bitcast_fusion.2), channel_id=1, replica_groups=mesh['sp'=16,'tp'=2] {'sp'}, dimensions={0}, use_global_device_ids=true | all-gather | bytes 69632 | tf_op jit(solution)/shard_map/all_gather | solution.py:18
  390.9 4.6 pad.227
  399.1 46.4 %all-gather = f32[16,1,1024]{2,1,0:T(1,128)S(1)} all-gather(f32[1,1,1024]{2,1,0:T(1,128)S(1)} %add_bitcast_fusion.3), channel_id=1, replica_groups=mesh['sp'=16,'tp'=2] {'sp'}, dimensions={0}, use_global_device_ids=true | all-gather | bytes 69632 | tf_op jit(solution)/shard_map/all_gather | solution.py:18
  445.8 8.5 %fusion.4 = bf16[256,4096]{1,0:T(8,128)(2,1)} fusion(bf16[2,1024,4096]{2,1,0:T(8,128)(2,1)} %all-gather.9.cloned.1.call-done, f32[256,1024]{1,0:T(8,128)} %pad.226, f32[256,1024]{1,0:T(8,128)} %pad.227, f32[256,1024]{1,0:T(8,128)} %pad.210, f32[256,1024]{1,0:T(8,128)} %pad.211, f32[1024]{0:T(1024)S(1)} %get-tuple-element.93), kind=kOutput, calls=%fused_computation.20 | convolution fusion | flops 2149842944 | bytes 14684160 | tf_op jit(solution)/shard_map/dot_general | solution.py:107
  454.4 20.7 %all-reduce.67.cloned.1.call-done = bf16[256,4096]{1,0:T(8,128)(2,1)} async-done(((bf16[256,4096]{1,0:T(8,128)(2,1)}), bf16[256,4096]{1,0:T(8,128)(2,1)}) %all-reduce.67.cloned.1.call-update) | async-done | bytes 2097168 | tf_op jit(solution)/shard_map/psum | solution.py:108
  477.7 5.8 fusion.23
  484.4 3.6 collective-permute-start.2
  504.2 4.2 multiply_multiply_fusion
  510.5 3.3 slice.717
  513.7 3.3 slice.715
  589.1 3.3 slice.771
  610.4 4.6 pad.243
  629.1 41.7 %all-gather.3 = f32[16,1,1024]{2,1,0:T(1,128)S(1)} all-gather(f32[1,1,1024]{2,1,0:T(1,128)S(1)} %add_bitcast_fusion), channel_id=1, replica_groups=mesh['sp'=16,'tp'=2] {'sp'}, dimensions={0}, use_global_device_ids=true | all-gather | bytes 69632 | tf_op jit(solution)/shard_map/all_gather | solution.py:18
  670.9 4.6 pad.259
  679.1 35.8 %all-gather.2 = f32[16,1,1024]{2,1,0:T(1,128)S(1)} all-gather(f32[1,1,1024]{2,1,0:T(1,128)S(1)} %add_bitcast_fusion.1), channel_id=1, replica_groups=mesh['sp'=16,'tp'=2] {'sp'}, dimensions={0}, use_global_device_ids=true | all-gather | bytes 69632 | tf_op jit(solution)/shard_map/all_gather | solution.py:18
  715.0 8.4 %fusion.5 = bf16[256,4096]{1,0:T(8,128)(2,1)} fusion(bf16[2,1024,4096]{2,1,0:T(8,128)(2,1)} %all-gather.9.cloned.1.call-done, f32[256,1024]{1,0:T(8,128)} %pad.258, f32[256,1024]{1,0:T(8,128)} %pad.259, f32[256,1024]{1,0:T(8,128)} %pad.242, f32[256,1024]{1,0:T(8,128)} %pad.243, f32[1024]{0:T(1024)S(1)} %get-tuple-element.94), kind=kOutput, calls=%fused_computation.21 | convolution fusion | flops 2149842944 | bytes 14684160 | tf_op jit(solution)/shard_map/dot_general | solution.py:107
  723.4 20.1 %all-reduce.69.cloned.1.call-done = bf16[256,4096]{1,0:T(8,128)(2,1)} async-done(((bf16[256,4096]{1,0:T(8,128)(2,1)}), bf16[256,4096]{1,0:T(8,128)(2,1)}) %all-reduce.69.cloned.1.call-update) | async-done | bytes 2097168 | tf_op jit(solution)/shard_map/psum | solution.py:108
  743.5 4.7 fusion.13
  (377 shorter events, 268.1 us)
Async XLA Ops:
  6.5 197.4 %copy-start = (bf16[256,4096]{1,0:T(8,128)(2,1)S(1)}, bf16[256,4096]{1,0:T(8,128)(2,1)}, u32[]{:S(2)}) copy-start(bf16[256,4096]{1,0:T(8,128)(2,1)} %param.16) | copy-start | bytes 6291460
  6.6 197.4 %all-gather.7.cloned.1.call-start = ((), (), s32[]{:S(2)}) async-start(), calls=%async_computation | async-start | bytes 17825792 | tf_op jit(solution)/shard_map/all_gather | solution.py:61
  7.3 438.5 %all-gather.9.cloned.1.call-start = ((), (), s32[]{:S(2)}) async-start(), calls=%async_computation.1 | async-start | bytes 17825792 | tf_op jit(solution)/shard_map/all_gather | solution.py:62
  8.1 467.1 %all-reduce.67.cloned.1.call-start = ((), (), s32[]{:S(2)}) async-start(), calls=%async_computation.2 | async-start | bytes 4194304 | tf_op jit(solution)/shard_map/psum | solution.py:108
  8.9 10.7 %collective-permute-start.1 = (bf16[3]{0:T(256)(128)(2,1)S(1)}, bf16[3]{0:T(256)(128)(2,1)S(1)}, u32[]{:S(2)}, u32[]{:S(2)}) collective-permute-start(bf16[3]{0:T(256)(128)(2,1)S(1)} %slice.605), channel_id=1, source_target_pairs={{0,2},{2,4},{4,6},{6,8},{8,10},{10,12},{12,14},{14,16},{16,18},{18... | collective-permute-start | bytes 26 | tf_op jit(solution)/shard_map/ppermute | solution.py:13
  209.8 4.3 collective-permute-start
  212.8 14.9 %copy-start.30 = (pred[256]{0:T(512)(128)(4,1)}, pred[256]{0:T(512)(128)(4,1)S(1)}, u32[]{:S(2)}) copy-start(pred[256]{0:T(512)(128)(4,1)S(1)} %get-tuple-element.209) | copy-start | bytes 772
  212.9 14.9 %copy-start.32 = (pred[256]{0:T(512)(128)(4,1)}, pred[256]{0:T(512)(128)(4,1)S(1)}, u32[]{:S(2)}) copy-start(pred[256]{0:T(512)(128)(4,1)S(1)} %get-tuple-element.211) | copy-start | bytes 772
  212.9 14.9 %copy-start.34 = (pred[256]{0:T(512)(128)(4,1)}, pred[256]{0:T(512)(128)(4,1)S(1)}, u32[]{:S(2)}) copy-start(pred[256]{0:T(512)(128)(4,1)S(1)} %get-tuple-element.212) | copy-start | bytes 772
  212.9 14.9 %copy-start.40 = (pred[256]{0:T(512)(128)(4,1)}, pred[256]{0:T(512)(128)(4,1)S(1)}, u32[]{:S(2)}) copy-start(pred[256]{0:T(512)(128)(4,1)S(1)} %get-tuple-element.210) | copy-start | bytes 772
  247.8 60.8 %copy-start.3 = (f32[256,1024]{1,0:T(8,128)S(1)}, f32[256,1024]{1,0:T(8,128)}, u32[]{:S(2)}) copy-start(f32[256,1024]{1,0:T(8,128)} %get-tuple-element.122) | copy-start | bytes 3145732
  302.4 21.8 %copy-start.9 = (f32[31,1024]{1,0:T(8,128)S(1)}, f32[31,1024]{1,0:T(8,128)}, u32[]{:S(2)}) copy-start(f32[31,1024]{1,0:T(8,128)} %slice.673) | copy-start | bytes 380932
  343.1 52.4 %copy-start.18 = (f32[1,1024]{1,0:T(1,128)S(1)}, f32[1,1024]{1,0:T(1,128)}, u32[]{:S(2)}) copy-start(f32[1,1024]{1,0:T(1,128)} %slice.822) | copy-start | bytes 12292
  345.7 49.8 %copy-start.6 = (f32[127,1024]{1,0:T(8,128)S(1)}, f32[127,1024]{1,0:T(8,128)}, u32[]{:S(2)}) copy-start(f32[127,1024]{1,0:T(8,128)} %get-tuple-element.128) | copy-start | bytes 1560580
  454.3 23.3 %copy-start.29 = (f32[1,4096]{1,0:T(1,128)S(1)}, f32[1,4096]{1,0:T(1,128)}, u32[]{:S(2)}) copy-start(f32[1,4096]{1,0:T(1,128)} %get-tuple-element.172) | copy-start | bytes 49156
  454.4 289.2 %all-reduce.69.cloned.1.call-start = ((), (), s32[]{:S(2)}) async-start(), calls=%async_computation.3 | async-start | bytes 4194304 | tf_op jit(solution)/shard_map/psum | solution.py:108
  477.7 12.9 %copy-start.11 = (f32[1,1,1024]{2,1,0:T(1,128)S(1)}, f32[1,1,1024]{2,1,0:T(1,128)}, u32[]{:S(2)}) copy-start(f32[1,1,1024]{2,1,0:T(1,128)} %get-tuple-element.159) | copy-start | bytes 12292
  477.7 12.9 %copy-start.12 = (f32[1,1,1024]{2,1,0:T(1,128)S(1)}, f32[1,1,1024]{2,1,0:T(1,128)}, u32[]{:S(2)}) copy-start(f32[1,1,1024]{2,1,0:T(1,128)} %get-tuple-element.160) | copy-start | bytes 12292
  477.7 12.9 %copy-start.13 = (f32[1,1,1024]{2,1,0:T(1,128)S(1)}, f32[1,1,1024]{2,1,0:T(1,128)}, u32[]{:S(2)}) copy-start(f32[1,1,1024]{2,1,0:T(1,128)} %get-tuple-element.165) | copy-start | bytes 12292
  484.4 5.0 collective-permute-start.2
  524.2 63.4 %copy-start.2 = (f32[256,1024]{1,0:T(8,128)S(1)}, f32[256,1024]{1,0:T(8,128)}, u32[]{:S(2)}) copy-start(f32[256,1024]{1,0:T(8,128)} %get-tuple-element.120) | copy-start | bytes 3145732
  581.4 22.8 %copy-start.10 = (f32[31,1024]{1,0:T(8,128)S(1)}, f32[31,1024]{1,0:T(8,128)}, u32[]{:S(2)}) copy-start(f32[31,1024]{1,0:T(8,128)} %slice.767) | copy-start | bytes 380932
  623.0 52.6 %copy-start.22 = (f32[1,1024]{1,0:T(1,128)S(1)}, f32[1,1024]{1,0:T(1,128)}, u32[]{:S(2)}) copy-start(f32[1,1024]{1,0:T(1,128)} %slice.881) | copy-start | bytes 12292
  625.6 50.0 %copy-start.7 = (f32[127,1024]{1,0:T(8,128)S(1)}, f32[127,1024]{1,0:T(8,128)}, u32[]{:S(2)}) copy-start(f32[127,1024]{1,0:T(8,128)} %get-tuple-element.124) | copy-start | bytes 1560580
  (26 other events, 232.4 us)
Sparse Core Ops, SparseCore 0:
  10.1 193.7 all-gather.6
  206.7 233.8 all-gather.8
  454.5 20.5 all-reduce.66
  723.5 19.9 all-reduce.68
where the time goes:
time: 762 us; the launch traced here: 755 us
  waiting for transfers between devices  229 us (30%)
  local copies, waits for them, and re-layouts  206 us (27%)
  blocking collectives  166 us (22%)
  other arithmetic  89.8 us (12%)
  matrix products  38.3 us (5%)
  between operations  14.2 us (2%)
  starting transfers between devices  11.6 us (2%)
    all_gather x1, waiting for transfers between devices, per_device(): lax.all_gather(in_weight, 'sp', axis=1, tiled=True)  184 us
    all_gather x4, blocking collectives, carried_in(): gathered = jax.tree.map(lambda a: lax.all_gather(a, axis), part)  166 us
    slice x104, local copies, waits for them, and re-layouts, per_device(): lax.associative_scan(combine, (decay_now, drive_term), axis=0)  145 us
    pad x56, local copies, waits for them, and re-layouts, per_device(): lax.associative_scan(combine, (decay_now, drive_term), axis=0)  42.5 us
    psum x2, waiting for transfers between devices, per_device(): lax.psum(partial_sum.astype(jnp.bfloat16), 'tp').astype(jnp.float32)  40.8 us
    add x26, other arithmetic, combine(): return (earlier[0] * following[0], following[0] * earlier[1] + following[1])  36.2 us
    dot_general x2, matrix products, per_device(): jnp.dot(hidden, whole_out[depth_at], preferred_element_type=jnp.float32)  16.9 us
    concatenate x27, other arithmetic, per_device(): lax.associative_scan(combine, (decay_now, drive_term), axis=0)  16 us
  transfers between devices with their start and end apart: 7, of which 5 were waited for; matrix products, arithmetic and copies ran while one was open for 21% of the time, Pallas kernels for 0%

commit v1 on v0

v1 whole, which is shorter than its diff:
```python
import functools
import jax
import jax.numpy as jnp
from jax import lax
from jax.experimental import pallas as pl
from jax.experimental.pallas import tpu as pltpu
from jax.sharding import Mesh, PartitionSpec as P

RG_C = 8.0
EPS = 0.1
SUB = 8
F32 = jnp.float32
BF16 = jnp.bfloat16
VMEM_LIMIT = 48 * 1024 * 1024


def vmem():
    return pl.BlockSpec(memory_space=pltpu.VMEM)


def params(**kw):
    return pltpu.CompilerParams(vmem_limit_bytes=VMEM_LIMIT, **kw)


def in_kernel(groups, adds, x_ref, *refs):
    y_refs, (gain_ref, w_ref), outs = refs[:adds], refs[adds : adds + 2], refs[adds + 2 :]
    if adds:
        new_ref, outs = outs[0], outs[1:]
    ss_ref, m_refs = outs[0], outs[1:]
    slices, rows, width = x_ref.shape
    lanes = min(width, 128)
    squares = jnp.zeros((rows, lanes), F32)
    scaled = []
    for z in range(slices):
        value = x_ref[z].astype(F32)
        if adds:
            summed = y_refs[0][z].astype(F32)
            for y_ref in y_refs[1:]:
                summed = summed + y_ref[z].astype(F32)
            rounded = (value + summed).astype(BF16)
            new_ref[z] = rounded
            value = rounded.astype(F32)
        square = value * value
        for low in range(0, width, lanes):
            squares = squares + square[:, low : low + lanes]
        scaled.append((value * gain_ref[z]).astype(BF16))
    for low in range(0, rows, 128):
        ss_ref[0, :, low : low + 128] = jnp.sum(squares[low : low + 128].T, axis=0, keepdims=True)
    for k in range(groups):
        total = jnp.dot(scaled[0], w_ref[0, k], preferred_element_type=F32)
        for z in range(1, slices):
            total = total + jnp.dot(scaled[z], w_ref[z, k], preferred_element_type=F32)
        m_refs[k][...] = total.astype(BF16)


def in_projection(x, ys, gain, w):
    slices, rows, width = x.shape
    groups, chans = w.shape[1], w.shape[3]
    tile = min(rows, 256)
    count = rows // tile
    row_block = pl.BlockSpec((slices, tile, width), lambda i: (0, i, 0))
    out_shape = [jax.ShapeDtypeStruct((count, 1, tile), F32)]
    out_specs = [pl.BlockSpec((1, 1, tile), lambda i: (i, 0, 0))]
    for _ in range(groups):
        out_shape.append(jax.ShapeDtypeStruct((rows, chans), BF16))
        out_specs.append(pl.BlockSpec((tile, chans), lambda i: (i, 0)))
    if ys:
        out_shape.insert(0, jax.ShapeDtypeStruct(x.shape, BF16))
        out_specs.insert(0, row_block)
    got = pl.pallas_call(
        functools.partial(in_kernel, groups, len(ys)),
        grid=(count,),
        in_specs=[row_block] * (1 + len(ys))
        + [
            pl.BlockSpec(gain.shape, lambda i: (0, 0, 0)),
            pl.BlockSpec(w.shape, lambda i: (0, 0, 0, 0)),
        ],
        out_specs=out_specs,
        out_shape=out_shape,
        compiler_params=params(),
        name="in_projection",
    )(x, *ys, gain, w)
    if ys:
        return got[0], got[1], got[2:]
    return x, got[0], got[1:]


def mix_kernel(groups, features, *refs):
    m_refs, s_refs, (mixed_ref, tail_ref) = refs[:groups], refs[groups : 2 * groups], refs[2 * groups :]
    rows, chans = mixed_ref.shape
    count, _, tile = s_refs[0].shape
    lanes = min(chans, 128)
    for n in range(count):
        stat = s_refs[0][n]
        for s_ref in s_refs[1:]:
            stat = stat + s_ref[n]
        factor = lax.rsqrt(stat * (1.0 / features) + EPS)
        for low in range(0, tile, 128):
            column = jnp.broadcast_to(factor[:, low : low + 128], (128, 128)).T
            at = n * tile + low
            for lane in range(0, chans, lanes):
                total = m_refs[0][at : at + 128, lane : lane + lanes].astype(F32)
                for m_ref in m_refs[1:]:
                    total = total + m_ref[at : at + 128, lane : lane + lanes].astype(F32)
                mixed_ref[at : at + 128, lane : lane + lanes] = (total * column[:, :lanes]).astype(BF16)
    last = mixed_ref[rows - 4 * SUB :, :].astype(F32)
    ends = [last[j * SUB + SUB - 1 : (j + 1) * SUB, :] for j in range(4)]
    tail_ref[...] = jnp.concatenate(ends + ends, axis=0)


def mix(pieces, stats, features):
    rows, chans = pieces[0].shape
    return pl.pallas_call(
        functools.partial(mix_kernel, len(pieces), features),
        in_specs=[vmem()] * (2 * len(pieces)),
        out_specs=[vmem(), vmem()],
        out_shape=[
            jax.ShapeDtypeStruct((rows, chans), BF16),
            jax.ShapeDtypeStruct((SUB, chans), F32),
        ],
        compiler_params=params(),
        name="mix",
    )(*pieces, *stats)


def recur_kernel(
    taps_count, mixed_ref, halo_ref, keep_ref, table_ref, gate_ref,
    cum_ref, state_ref, head_ref, ext_ref, conv_ref, pre_ref,
):
    rows, chans = mixed_ref.shape
    lead = (taps_count - 1) * SUB
    tile = 64
    ext_ref[lead:, :] = mixed_ref[...].astype(F32)
    for j in range(taps_count - 1):
        back = taps_count - 1 - j
        end = ext_ref[lead + rows - back * SUB : lead + rows - (back - 1) * SUB, :]
        ext_ref[j * SUB : (j + 1) * SUB, :] = jnp.concatenate(
            [halo_ref[4 - back : 5 - back, :], end[: SUB - 1]], axis=0
        )

    def conv(step, _):
        at = pl.multiple_of(step * tile, tile)
        total = table_ref[taps_count : taps_count + 1, :] + table_ref[0:1, :] * ext_ref[
            pl.ds(at + lead, tile), :
        ]
        for lag in range(1, taps_count):
            total = total + keep_ref[pl.ds(at, tile), lag - 1 : lag] * (
                table_ref[lag : lag + 1, :] * ext_ref[pl.ds(at + lead - lag * SUB, tile), :]
            )
        conv_ref[pl.ds(at, tile), :] = total.astype(BF16)
        return 0

    lax.fori_loop(0, rows // tile, conv, 0)
    pre_ref[...] = jnp.dot(conv_ref[...], gate_ref[...], preferred_element_type=F32)
    base = taps_count + 1

    def scan(step, carry):
        cum, state = carry
        at = pl.multiple_of(step * tile, tile)
        recur_rate = jax.nn.sigmoid(pre_ref[pl.ds(at, tile), :chans] + table_ref[base : base + 1, :])
        input_rate = jax.nn.sigmoid(
            pre_ref[pl.ds(at, tile), chans:] + table_ref[base + 1 : base + 2, :]
        )
        log_decay = table_ref[base + 2 : base + 3, :] * recur_rate
        decay = jnp.exp(log_decay)
        twice = 2.0 * log_decay
        near = -twice * (1.0 + twice * (0.5 + twice * (1.0 / 6.0 + twice * (1.0 / 24.0))))
        rest = jnp.where(twice > -0.03, near, 1.0 - decay * decay)
        drive = jnp.sqrt(jnp.maximum(rest, 0.0)) * (
            input_rate * conv_ref[pl.ds(at, tile), :].astype(F32)
        )
        decay = keep_ref[pl.ds(at, tile), 0:1] * decay
        cums, states = [], []
        for i in range(tile // SUB):
            now = decay[i * SUB : (i + 1) * SUB]
            cum = cum * now
            state = state * now + drive[i * SUB : (i + 1) * SUB]
            cums.append(cum)
            states.append(state)
        cum_ref[pl.ds(at, tile), :] = jnp.concatenate(cums, axis=0)
        state_ref[pl.ds(at, tile), :] = jnp.concatenate(states, axis=0)
        return cum, state

    cum, state = lax.fori_loop(
        0, rows // tile, scan, (jnp.ones((SUB, chans), F32), jnp.zeros((SUB, chans), F32))
    )
    decays, states = [jnp.ones((1, chans), F32)], [jnp.zeros((1, chans), F32)]
    for s in range(SUB):
        decays.append(decays[-1] * cum[s : s + 1])
        states.append(states[-1] * cum[s : s + 1] + state[s : s + 1])
    head_ref[0:SUB, :] = jnp.concatenate(decays[:SUB], axis=0)
    head_ref[SUB : 2 * SUB, :] = jnp.concatenate(states[:SUB], axis=0)
    head_ref[2 * SUB :, :] = jnp.concatenate([decays[SUB], states[SUB]] * (SUB // 2), axis=0)


def recur(mixed, halo, keep, table, gate, taps_count):
    rows, chans = mixed.shape
    return pl.pallas_call(
        functools.partial(recur_kernel, taps_count),
        in_specs=[vmem()] * 5,
        out_specs=[vmem()] * 3,
        out_shape=[
            jax.ShapeDtypeStruct((rows, chans), F32),
            jax.ShapeDtypeStruct((rows, chans), F32),
            jax.ShapeDtypeStruct((3 * SUB, chans), F32),
        ],
        scratch_shapes=[
            pltpu.VMEM((rows + (taps_count - 1) * SUB, chans), F32),
            pltpu.VMEM((rows, chans), BF16),
            pltpu.VMEM((rows, 2 * chans), F32),
        ],
        compiler_params=params(),
        name="recur",
    )(mixed, halo, keep, table, gate)


def hidden_kernel(cum_ref, state_ref, head_ref, *refs):
    segment_refs, hidden_ref = refs[:-1], refs[-1]
    rows, chans = cum_ref.shape
    carried = jnp.zeros((1, chans), F32)
    for segment_ref in segment_refs:
        carried = carried * segment_ref[0:1, :] + segment_ref[1:2, :]
    entering = head_ref[SUB : 2 * SUB, :] + head_ref[0:SUB, :] * carried
    tile = 64
    wide = jnp.concatenate([entering] * (tile // SUB), axis=0)

    def step_of(step, _):
        at = pl.multiple_of(step * tile, tile)
        hidden_ref[pl.ds(at, tile), :] = (
            state_ref[pl.ds(at, tile), :] + cum_ref[pl.ds(at, tile), :] * wide
        ).astype(BF16)
        return 0

    lax.fori_loop(0, rows // tile, step_of, 0)


def hidden_of(cum, state, head, segments):
    return pl.pallas_call(
        hidden_kernel,
        in_specs=[vmem()] * (3 + len(segments)),
        out_specs=vmem(),
        out_shape=jax.ShapeDtypeStruct(cum.shape, BF16),
        compiler_params=params(),
        name="hidden",
    )(cum, state, head, *segments)


def out_kernel(groups, *refs):
    h_refs, w_ref, y_ref = refs[:groups], refs[groups], refs[groups + 1]
    for z in range(w_ref.shape[0]):
        total = jnp.dot(h_refs[0][...], w_ref[z, 0], preferred_element_type=F32)
        for k in range(1, groups):
            total = total + jnp.dot(h_refs[k][...], w_ref[z, k], preferred_element_type=F32)
        y_ref[z] = total.astype(BF16)


def out_projection(pieces, w):
    rows, chans = pieces[0].shape
    slices, groups, _, width = w.shape
    tile = min(rows, 256)
    return pl.pallas_call(
        functools.partial(out_kernel, groups),
        grid=(rows // tile,),
        in_specs=[pl.BlockSpec((tile, chans), lambda i: (i, 0))] * groups
        + [pl.BlockSpec(w.shape, lambda i: (0, 0, 0, 0))],
        out_specs=pl.BlockSpec((slices, tile, width), lambda i: (0, i, 0)),
        out_shape=jax.ShapeDtypeStruct((slices, rows, width), BF16),
        compiler_params=params(),
        name="out_projection",
    )(*pieces, w)


def swapped(value, axis, count, k):
    return lax.ppermute(value, axis, [(i, i ^ k) for i in range(count)])


def passed_along(value, axis, count, distance):
    return lax.ppermute(value, axis, [(i, i + distance) for i in range(count - distance)])


def per_device(
    tokens, documents, norm_gain, in_weight, conv_taps, conv_bias, recur_gate, input_gate,
    recur_bias, input_bias, decay_param, out_weight,
):
    outer, inner, pair = lax.axis_size("so"), lax.axis_size("si"), lax.axis_size("tp")
    place = lax.axis_index("si")
    own_rows, features = tokens.shape
    layers, width, chan_width = in_weight.shape
    taps_count = conv_taps.shape[1]
    block_dim = recur_gate.shape[2]
    rows = own_rows * inner
    steps = rows // SUB
    parts = own_rows // steps
    chans = chan_width // inner
    blocks = chans // block_dim
    others = [place ^ k for k in range(inner)]

    def in_piece(layer):
        split = in_weight[layer].reshape(width, inner, chans)
        return jnp.stack([lax.dynamic_index_in_dim(split, o, 1, False) for o in others])

    def out_piece(layer):
        split = out_weight[layer].reshape(inner, chans, width)
        return jnp.stack([lax.dynamic_index_in_dim(split, o, 0, False) for o in others])

    whole_in, whole_out = [], []
    for layer in range(layers):
        whole_in.append(lax.all_gather(in_piece(layer), "so", axis=0))
        whole_out.append(lax.all_gather(out_piece(layer), "so", axis=0))

    send = tokens.reshape(parts, steps, outer, inner, width).transpose(3, 2, 1, 0, 4)
    got = lax.all_to_all(send, "si", 0, 0, tiled=True)
    state_x = got.transpose(1, 2, 0, 3, 4).reshape(outer, rows, width)

    docs = documents.astype(F32)
    received = jnp.stack([docs] + [swapped(docs, "si", inner, k) for k in range(1, inner)])
    docs = jnp.concatenate([lax.dynamic_index_in_dim(received, place ^ j, 0, False) for j in range(inner)])
    before = passed_along(docs[rows - taps_count + 1 :] + 1.0, "so", outer, 1) - 1.0
    ext_docs = jnp.concatenate([before, docs])
    keeps = [
        (ext_docs[taps_count - 1 - lag : taps_count - 1 - lag + rows] == docs).astype(F32)
        for lag in range(1, taps_count)
    ]
    keep = jnp.stack(keeps, axis=-1).reshape(SUB, steps, taps_count - 1)
    keep = keep.transpose(1, 0, 2).reshape(rows, taps_count - 1)

    def own(values):
        return lax.dynamic_slice_in_dim(values, place * chans, chans, -1)

    def diagonal(gate):
        gate = lax.dynamic_slice_in_dim(gate, place * blocks, blocks, 1)
        eye = jnp.eye(blocks, dtype=BF16)
        full = gate[:, :, :, None, :] * eye[None, :, None, :, None]
        return full.reshape(layers, chans, chans)

    gates = jnp.concatenate([diagonal(recur_gate), diagonal(input_gate)], axis=-1)
    slope = -RG_C * jax.nn.softplus(-own(decay_param))
    rows_of = [own(conv_bias), own(recur_bias), own(input_bias), slope]
    table = jnp.concatenate([own(conv_taps)] + [r[:, None] for r in rows_of], axis=1)
    gain = lax.dynamic_index_in_dim(norm_gain.reshape(layers, outer, inner, width), place, 2, True)

    addends = []
    for layer in range(layers):
        state_x, stat, partials = in_projection(state_x, addends, gain[layer], whole_in[layer])
        pieces = [partials[0]] + [swapped(partials[k], "si", inner, k) for k in range(1, inner)]
        stats = [stat] + [swapped(stat, "si", inner, k) for k in range(1, inner)]
        mixed, tail = mix(pieces, stats, features)
        halo = passed_along(tail, "so", outer, 1)
        cum, state, head = recur(mixed, halo, keep, table[layer], gates[layer], taps_count)
        segment = head[2 * SUB :]
        if outer <= 4:
            segments = [passed_along(segment, "so", outer, d) for d in range(outer - 1, 0, -1)]
        else:
            gathered = lax.all_gather(segment, "so")
            earlier = (jnp.arange(outer) < lax.axis_index("so"))[:, None, None]
            first = jnp.arange(SUB)[:, None] % 2 == 0
            gathered = jnp.where(earlier, gathered, jnp.where(first, 1.0, 0.0))
            segments = [gathered[d] for d in range(outer)]
        hidden = hidden_of(cum, state, head, segments)
        pieces = [hidden] + [swapped(hidden, "si", inner, k) for k in range(1, inner)]
        partial = out_projection(pieces, whole_out[layer])
        if pair == 2:
            addends = [partial, swapped(partial, "tp", pair, 1)]
        else:
            addends = [lax.psum(partial, "tp")]

    summed = addends[0].astype(F32)
    for addend in addends[1:]:
        summed = summed + addend.astype(F32)
    state_x = (state_x.astype(F32) + summed).astype(BF16)
    send = state_x.reshape(outer, steps, inner, parts, width).transpose(2, 3, 1, 0, 4)
    got = lax.all_to_all(send, "si", 0, 0, tiled=True)
    return got.transpose(1, 2, 3, 0, 4).reshape(own_rows, features)


def solution(mesh):
    count = mesh.shape["sp"]
    inner = 4
    split = Mesh(
        mesh.devices.reshape(count // inner, inner, mesh.shape["tp"]), ("so", "si", "tp")
    )
    sp = ("so", "si")
    return jax.shard_map(
        per_device,
        mesh=split,
        in_specs=(
            P(sp, None),
            P(sp),
            P(),
            P(None, sp, "tp"),
            P(None, None, "tp"),
            P(None, "tp"),
            P(None, "tp", None, None),
            P(None, "tp", None, None),
            P(None, "tp"),
            P(None, "tp"),
            P(None, "tp"),
            P(None, "tp", sp),
        ),
        out_specs=P(sp, None),
        check_vma=False,
    )
```

time: 762 us -> 285 us (0.37)
  local copies, waits for them, and re-layouts: 206 us -> 35.2 us
  blocking collectives: 166 us -> 28.4 us
  waiting for transfers between devices: 229 us -> 112 us
  other arithmetic: 89.8 us -> 6.89 us
  starting transfers between devices: 11.6 us -> 58.4 us
  matrix products: 38.3 us -> 0 us
  Pallas kernels: 0 us -> 29.7 us
    all_gather x2 -> x4, waiting for transfers between devices: 184 us -> 4.44 us  [the longest x2 4.43 us: per_device(): whole_in.append(lax.all_gather(in_piece(layer), 'so', axis=0))]
    all_gather x4 -> x0, blocking collectives: 166 us -> none  [carried_in(): gathered = jax.tree.map(lambda a: lax.all_gather(a, axis), part)]
    slice x112 -> x4, local copies, waits for them, and re-layouts: 148 us -> 1.35 us  [the longest x1 1.28 us: in_piece(): split = in_weight[layer].reshape(width, inner, chans)]
    ppermute x3 -> x32, waiting for transfers between devices: 2.59 us -> 107 us  [the longest x23 102 us: swapped(): return lax.ppermute(value, axis, [(i, i ^ k) for i in range(count)])]
    add x53 -> x1, other arithmetic: 45 us -> 0.08 us  [per_device(): docs[rows - taps_count + 1:] + 1.0]
    pad x56 -> x0, local copies, waits for them, and re-layouts: 42.5 us -> none  [per_device(): lax.associative_scan(combine, (decay_now, drive_term), axis=0)]
    ppermute x3 -> x32, starting transfers between devices: 11.5 us -> 53 us  [the longest x9 27.9 us: passed_along(): lax.ppermute(value, axis, [(i, i + distance) for i in range(count - dista...]
    psum x2 -> x0, waiting for transfers between devices: 40.8 us -> none  [per_device(): lax.psum(partial_sum.astype(jnp.bfloat16), 'tp').astype(jnp.float32)]
  transfers between devices with their start and end apart: 7 -> 37, of which waited for: 5 -> 16; matrix products, arithmetic and copies ran while one was open for 21% -> 7% of each run, Pallas kernels for 0% -> 9%
where the time goes in v1:
time: 285 us; the launch traced here: 284 us
  waiting for transfers between devices  112 us (39%)
  starting transfers between devices  58.4 us (20%)
  local copies, waits for them, and re-layouts  35.2 us (12%)
  Pallas kernels  29.7 us (10%)
  blocking collectives  28.4 us (10%)
  between operations  13.7 us (5%)
  other arithmetic  6.89 us (2%)
    ppermute x23, waiting for transfers between devices, swapped(): return lax.ppermute(value, axis, [(i, i ^ k) for i in range(count)])  102 us
    all_to_all x1, blocking collectives, per_device(): got = lax.all_to_all(send, 'si', 0, 0, tiled=True)  28.4 us
    ppermute x9, starting transfers between devices, passed_along(): lax.ppermute(value, axis, [(i, i + distance) for i in range(count - dista...  27.9 us
    ppermute x23, starting transfers between devices, swapped(): return lax.ppermute(value, axis, [(i, i ^ k) for i in range(count)])  25.1 us
    pallas_call x2, Pallas kernels, in_projection(): pl.pallas_call(functools.partial(in_kernel, groups, len(ys)), grid=(count...  12 us
    pallas_call x2, Pallas kernels, out_projection(): pl.pallas_call(functools.partial(out_kernel, groups), grid=(rows // tile,...  9.32 us
    pallas_call x2, Pallas kernels, recur(): pl.pallas_call(functools.partial(recur_kernel, taps_count), in_specs=[vme...  7.34 us
    unnamed x40, local copies, waits for them, and re-layouts  7.34 us
  transfers between devices with their start and end apart: 37, of which 16 were waited for; matrix products, arithmetic and copies ran while one was open for 7% of the time, Pallas kernels for 9%

profile of v1, /device:TPU:0, one launch (start us, length us, event | category | flops | bytes accessed | tf_op | source)
XLA Modules:
  0.0 284.0 jit_solution(18173770841346101218)
XLA Ops:
  13.0 3.3 %reshape.201 = bf16[2,128,4,4,256]{4,3,2,1,0:T(4,128)(2,1)S(1)} reshape(bf16[256,4096]{1,0:T(8,128)(2,1)} %param.12) | data formatting | bytes 4194304 | tf_op jit(solution)/shard_map/reshape | solution.py:311
  16.3 3.5 %copy.44 = bf16[4,4,128,2,256]{4,3,2,1,0:T(2,128)(2,1)} copy(bf16[4,4,128,2,256]{4,0,1,2,3:T(4,128)(2,1)S(1)} %bitcast.68) | data formatting | bytes 4194304 | tf_op jit(solution)/shard_map/transpose | solution.py:311
  19.8 5.3 %all-to-all-start = ((bf16[4,4,128,2,256]{4,3,2,1,0:T(2,128)(2,1)}), bf16[4,4,128,2,256]{4,3,2,1,0:T(2,128)(2,1)S(1)}, u32[]{:S(2)}, u32[]{:S(2)}) async-start(bf16[4,4,128,2,256]{4,3,2,1,0:T(2,128)(2,1)} %copy.44), calls=%async_computation | async-start | bytes 4194304 | tf_op jit(solution)/shard_map/all_to_all | solution.py:312
  32.8 17.3 %collective-permute-done.7 = f32[256]{0:T(256)S(1)} collective-permute-done((f32[256]{0:T(256)S(1)}, f32[256]{0:T(256)S(1)}, u32[]{:S(2)}, u32[]{:S(2)}) %collective-permute-start.7) | collective-permute-done | bytes 1056 | tf_op jit(solution)/shard_map/ppermute | solution.py:274
  51.0 3.6 %collective-permute-start.10 = (f32[3]{0:T(128)S(1)}, f32[3]{0:T(128)S(1)}, u32[]{:S(2)}, u32[]{:S(2)}) collective-permute-start(f32[3]{0:T(128)S(1)} %fusion.11), channel_id=1, source_target_pairs={{0,8},{8,16},{16,24},{1,9},{9,17},{17,25},{2,10},{10,18},{18,26},{... | collective-permute-start | bytes 44 | tf_op jit(solution)/shard_map/ppermute | solution.py:278
  60.2 6.0 %in_projection.2 = (f32[4,1,256]{2,1,0:T(1,128)S(1)}, bf16[1024,256]{1,0:T(8,128)(2,1)S(1)}, bf16[1024,256]{1,0:T(8,128)(2,1)}, bf16[1024,256]{1,0:T(8,128)(2,1)}, bf16[1024,256]{1,0:T(8,128)(2,1)}) custom-call(bf16[4,1024,256]{2,1,0:T(8,128)(2,1)S(1)} %reshape.202.x_ref, f32[4,1,256]{2,1,0:T(1,128)S(1)} %get-tuple-element.72.refs_0_, ...), custom_call_target="tpu_custom_call" | custom-call | tf_op jit(solution)/shard_map/in_projection/pallas_call | solution.py:70
  71.0 19.3 %collective-permute-done.3.refs_5_ = f32[4,1,256]{2,1,0:T(1,128)S(1)} collective-permute-done((f32[4,1,256]{2,1,0:T(1,128)S(1)}, f32[4,1,256]{2,1,0:T(1,128)S(1)}, u32[]{:S(2)}, u32[]{:S(2)}) %collective-permute-start.3) | collective-permute-done | bytes 4128 | tf_op jit(solution)/shard_map/ppermute | solution.py:274
  91.1 3.7 %collective-permute-done.5.refs_7_ = f32[4,1,256]{2,1,0:T(1,128)S(1)} collective-permute-done((f32[4,1,256]{2,1,0:T(1,128)S(1)}, f32[4,1,256]{2,1,0:T(1,128)S(1)}, u32[]{:S(2)}, u32[]{:S(2)}) %collective-permute-start.5) | collective-permute-done | bytes 4128 | tf_op jit(solution)/shard_map/ppermute | solution.py:274
  99.7 3.7 %recur.2 = (f32[1024,256]{1,0:T(8,128)S(1)}, f32[1024,256]{1,0:T(8,128)S(1)}, f32[24,256]{1,0:T(8,128)S(1)}) custom-call(bf16[1024,256]{1,0:T(8,128)(2,1)S(1)} %get-tuple-element.31.mixed_ref, f32[8,256]{1,0:T(8,128)S(1)} %collective-permute-done.6.halo_ref, f32[1024,3]{1,0:T(8,128)S(1)} %bitcast.63, f32[8,256]{1,0:T(8,128)S(1)} %get-tuple-element.74.table_ref, ...), custom_call_target="tpu_custom_call" | custom-call | tf_op jit(solution)/shard_map/recur/pallas_call | solution.py:198
  103.4 5.4 %collective-permute-start.11 = (f32[8,256]{1,0:T(8,128)S(1)}, f32[8,256]{1,0:T(8,128)S(1)}, u32[]{:S(2)}, u32[]{:S(2)}) collective-permute-start(f32[8,256]{1,0:T(8,128)S(1)} %slice.66), channel_id=1, source_target_pairs={{0,24},{1,25},{2,26},{3,27},{4,28},{5,29},{6,30},{7,31}} | collective-permute-start | bytes 24584 | tf_op jit(solution)/shard_map/ppermute | solution.py:278
  117.7 11.3 %collective-permute-done.14.refs_1_ = bf16[1024,256]{1,0:T(8,128)(2,1)S(1)} collective-permute-done((bf16[1024,256]{1,0:T(8,128)(2,1)S(1)}, bf16[1024,256]{1,0:T(8,128)(2,1)S(1)}, u32[]{:S(2)}, u32[]{:S(2)}) %collective-permute-start.14) | collective-permute-done | bytes 524320 | tf_op jit(solution)/shard_map/ppermute | solution.py:274
  129.8 5.7 %collective-permute-done.15.refs_2_ = bf16[1024,256]{1,0:T(8,128)(2,1)S(1)} collective-permute-done((bf16[1024,256]{1,0:T(8,128)(2,1)S(1)}, bf16[1024,256]{1,0:T(8,128)(2,1)S(1)}, u32[]{:S(2)}, u32[]{:S(2)}) %collective-permute-start.15) | collective-permute-done | bytes 524320 | tf_op jit(solution)/shard_map/ppermute | solution.py:274
  140.3 4.6 %out_projection.2.refs_0_ = bf16[4,1024,256]{2,1,0:T(8,128)(2,1)S(1)} custom-call(bf16[1024,256]{1,0:T(8,128)(2,1)S(1)} %hidden.2.refs_0_, bf16[1024,256]{1,0:T(8,128)(2,1)S(1)} %copy-done.7, bf16[1024,256]{1,0:T(8,128)(2,1)S(1)} %copy-done.9, bf16[1024,256]{1,0:T(8,128)(2,1)S(1)} %copy-done.11, bf16[4,4,256,256]{3,2,1,0:T(8,128)(2,1)} %bitcast.69), custom_call_target="tpu_custom_call" | custom-call | tf_op jit(solution)/shard_map/out_projection/pallas_call | solution.py:261
  146.1 4.4 %all-gather.13.cloned.1.call-done = bf16[16,256,256]{2,1,0:T(8,128)(2,1)} async-done(((bf16[4,256,256]{2,1,0:T(8,128)(2,1)}), bf16[16,256,256]{2,1,0:T(8,128)(2,1)}) %all-gather.13.cloned.1.call-update) | async-done | bytes 2097168 | tf_op jit(solution)/shard_map/all_gather | solution.py:308
  150.5 6.0 %in_projection.3 = (bf16[4,1024,256]{2,1,0:T(8,128)(2,1)S(1)}, f32[4,1,256]{2,1,0:T(1,128)S(1)}, bf16[1024,256]{1,0:T(8,128)(2,1)S(1)}, bf16[1024,256]{1,0:T(8,1...) custom-call(bf16[4,1024,256]{2,1,0:T(8,128)(2,1)} %copy-done.2, ...), custom_call_target="tpu_custom_call" | custom-call | tf_op jit(solution)/shard_map/in_projection/pallas_call | solution.py:70
  164.2 18.4 %collective-permute-done.21.refs_5_ = f32[4,1,256]{2,1,0:T(1,128)S(1)} collective-permute-done((f32[4,1,256]{2,1,0:T(1,128)S(1)}, f32[4,1,256]{2,1,0:T(1,128)S(1)}, u32[]{:S(2)}, u32[]{:S(2)}) %collective-permute-start.21) | collective-permute-done | bytes 4128 | tf_op jit(solution)/shard_map/ppermute | solution.py:274
  187.5 3.1 %collective-permute-start.24 = (f32[8,256]{1,0:T(8,128)S(1)}, f32[8,256]{1,0:T(8,128)S(1)}, u32[]{:S(2)}, u32[]{:S(2)}) collective-permute-start(f32[8,256]{1,0:T(8,128)S(1)} %get-tuple-element.43), channel_id=1, source_target_pairs={{0,8},{8,16},{16,24},{1,9},{9,17},{17,25},{2,10},{10,18},{18,26},{... | collective-permute-start | bytes 24584 | tf_op jit(solution)/shard_map/ppermute | solution.py:278
  192.1 3.7 %recur.3 = (f32[1024,256]{1,0:T(8,128)S(1)}, f32[1024,256]{1,0:T(8,128)S(1)}, f32[24,256]{1,0:T(8,128)S(1)}) custom-call(bf16[1024,256]{1,0:T(8,128)(2,1)S(1)} %get-tuple-element.42.mixed_ref, f32[8,256]{1,0:T(8,128)S(1)} %collective-permute-done.24.halo_ref, f32[1024,3]{1,0:T(8,128)S(1)} %bitcast.64, f32[8,256]{1,0:T(8,128)S(1)} %get-tuple-element.73.table_ref, ...), custom_call_target="tpu_custom_call" | custom-call | tf_op jit(solution)/shard_map/recur/pallas_call | solution.py:198
  195.8 5.0 %collective-permute-start.25 = (f32[8,256]{1,0:T(8,128)S(1)}, f32[8,256]{1,0:T(8,128)S(1)}, u32[]{:S(2)}, u32[]{:S(2)}) collective-permute-start(f32[8,256]{1,0:T(8,128)S(1)} %slice.72), channel_id=1, source_target_pairs={{0,24},{1,25},{2,26},{3,27},{4,28},{5,29},{6,30},{7,31}} | collective-permute-start | bytes 24584 | tf_op jit(solution)/shard_map/ppermute | solution.py:278
  209.7 11.3 %collective-permute-done.28.refs_1_ = bf16[1024,256]{1,0:T(8,128)(2,1)S(1)} collective-permute-done((bf16[1024,256]{1,0:T(8,128)(2,1)S(1)}, bf16[1024,256]{1,0:T(8,128)(2,1)S(1)}, u32[]{:S(2)}, u32[]{:S(2)}) %collective-permute-start.28) | collective-permute-done | bytes 524320 | tf_op jit(solution)/shard_map/ppermute | solution.py:274
  221.0 7.8 %collective-permute-done.29.refs_2_ = bf16[1024,256]{1,0:T(8,128)(2,1)S(1)} collective-permute-done((bf16[1024,256]{1,0:T(8,128)(2,1)S(1)}, bf16[1024,256]{1,0:T(8,128)(2,1)S(1)}, u32[]{:S(2)}, u32[]{:S(2)}) %collective-permute-start.29) | collective-permute-done | bytes 524320 | tf_op jit(solution)/shard_map/ppermute | solution.py:274
  228.8 4.7 %out_projection.3 = bf16[4,1024,256]{2,1,0:T(8,128)(2,1)S(1)} custom-call(bf16[1024,256]{1,0:T(8,128)(2,1)S(1)} %hidden.3.refs_0_, bf16[1024,256]{1,0:T(8,128)(2,1)S(1)} %collective-permute-done.28.refs_1_, bf16[1024,256]{1,0:T(8,128)(2,1)S(1)} %collective-permute-done.29.refs_2_, bf16[1024,256]{1,0:T(8,128)(2,1)S(1)} %collective-permute-done.30.refs_3_, ...), custom_call_target="tpu_custom_call" | custom-call | tf_op jit(solution)/shard_map/out_projection/pallas_call | solution.py:261
  233.6 4.1 %collective-permute-done.31 = bf16[4,1024,256]{2,1,0:T(8,128)(2,1)S(1)} collective-permute-done((bf16[4,1024,256]{2,1,0:T(8,128)(2,1)S(1)}, bf16[4,1024,256]{2,1,0:T(8,128)(2,1)S(1)}, u32[]{:S(2)}, u32[]{:S(2)}) %collective-permute-start.31) | collective-permute-done | bytes 2097184 | tf_op jit(solution)/shard_map/ppermute | solution.py:274
  244.6 28.4 %all_to_all.10 = bf16[4,2,128,4,256]{4,1,2,3,0:T(2,128)(2,1)S(1)} all-to-all(bf16[4,2,128,4,256]{4,1,2,3,0:T(2,128)(2,1)S(1)} %bitcast.66), channel_id=1, replica_groups=mesh['so'=4,'si'=4,'tp'=2] {'si'}, dimensions={0} | all-to-all | bytes 4194304 | tf_op jit(solution)/shard_map/all_to_all | solution.py:372
  (162 shorter events, 80.6 us)
Async XLA Ops:
  6.5 53.7 %all-gather.9.cloned.1.call-start = ((), (), s32[]{:S(2)}) async-start(), calls=%async_computation.2 | async-start | bytes 2621440 | tf_op jit(solution)/shard_map/all_gather | solution.py:308
  9.7 107.9 %all-gather.11.cloned.1.call-start = ((), (), s32[]{:S(2)}) async-start(), calls=%async_computation.3 | async-start | bytes 2621440 | tf_op jit(solution)/shard_map/all_gather | solution.py:309
  11.6 138.9 %all-gather.13.cloned.1.call-start = ((), (), s32[]{:S(2)}) async-start(), calls=%async_computation.4 | async-start | bytes 2621440 | tf_op jit(solution)/shard_map/all_gather | solution.py:308
  19.8 34.9 %all-to-all-start = ((bf16[4,4,128,2,256]{4,3,2,1,0:T(2,128)(2,1)}), bf16[4,4,128,2,256]{4,3,2,1,0:T(2,128)(2,1)S(1)}, u32[]{:S(2)}, u32[]{:S(2)}) async-start(bf16[4,4,128,2,256]{4,3,2,1,0:T(2,128)(2,1)} %copy.44), calls=%async_computation | async-start | bytes 4194304 | tf_op jit(solution)/shard_map/all_to_all | solution.py:312
  25.1 184.6 %all-gather.15.cloned.1.call-start = ((), (), s32[]{:S(2)}) async-start(), calls=%async_computation.5 | async-start | bytes 2621440 | tf_op jit(solution)/shard_map/all_gather | solution.py:309
  25.1 24.9 %collective-permute-start.7 = (f32[256]{0:T(256)S(1)}, f32[256]{0:T(256)S(1)}, u32[]{:S(2)}, u32[]{:S(2)}) collective-permute-start(f32[256]{0:T(256)S(1)} %convert_element_type.43), channel_id=1, source_target_pairs={{0,2},{2,0},{4,6},{6,4},{1,3},{3,1},{5,7},{7,5},{8,10},{10,8},{12,... | collective-permute-start | bytes 3080 | tf_op jit(solution)/shard_map/ppermute | solution.py:274
  27.2 22.8 %collective-permute-start.8 = (f32[256]{0:T(256)S(1)}, f32[256]{0:T(256)S(1)}, u32[]{:S(2)}, u32[]{:S(2)}) collective-permute-start(f32[256]{0:T(256)S(1)} %convert_element_type.43), channel_id=1, source_target_pairs={{0,4},{2,6},{4,0},{6,2},{1,5},{3,7},{5,1},{7,3},{8,12},{10,14},{12... | collective-permute-start | bytes 3080 | tf_op jit(solution)/shard_map/ppermute | solution.py:274
  28.7 22.2 %collective-permute-start.9 = (f32[256]{0:T(256)S(1)}, f32[256]{0:T(256)S(1)}, u32[]{:S(2)}, u32[]{:S(2)}) collective-permute-start(f32[256]{0:T(256)S(1)} %convert_element_type.43), channel_id=1, source_target_pairs={{0,6},{2,4},{4,2},{6,0},{1,7},{3,5},{5,3},{7,1},{8,14},{10,12},{12... | collective-permute-start | bytes 3080 | tf_op jit(solution)/shard_map/ppermute | solution.py:274
  51.0 19.3 %collective-permute-start.10 = (f32[3]{0:T(128)S(1)}, f32[3]{0:T(128)S(1)}, u32[]{:S(2)}, u32[]{:S(2)}) collective-permute-start(f32[3]{0:T(128)S(1)} %fusion.11), channel_id=1, source_target_pairs={{0,8},{8,16},{16,24},{1,9},{9,17},{17,25},{2,10},{10,18},{18,26},{... | collective-permute-start | bytes 44 | tf_op jit(solution)/shard_map/ppermute | solution.py:278
  66.2 28.6 %collective-permute-start = (bf16[1024,256]{1,0:T(8,128)(2,1)}, bf16[1024,256]{1,0:T(8,128)(2,1)S(1)}, u32[]{:S(2)}, u32[]{:S(2)}) collective-permute-start(bf16[1024,256]{1,0:T(8,128)(2,1)} %get-tuple-element.27), channel_id=1, source_target_pairs={{0,2},{2,0},{4,6},{6,4},{1,3},{3,1},{5,7},{7,5},{8,10},{10,8},{12,... | collective-permute-start | bytes 1572872 | tf_op jit(solution)/shard_map/ppermute | solution.py:274
  66.8 28.0 %collective-permute-start.1 = (bf16[1024,256]{1,0:T(8,128)(2,1)}, bf16[1024,256]{1,0:T(8,128)(2,1)S(1)}, u32[]{:S(2)}, u32[]{:S(2)}) collective-permute-start(bf16[1024,256]{1,0:T(8,128)(2,1)} %get-tuple-element.28), channel_id=1, source_target_pairs={{0,4},{2,6},{4,0},{6,2},{1,5},{3,7},{5,1},{7,3},{8,12},{10,14},{12... | collective-permute-start | bytes 1572872 | tf_op jit(solution)/shard_map/ppermute | solution.py:274
  67.3 27.5 %collective-permute-start.2 = (bf16[1024,256]{1,0:T(8,128)(2,1)}, bf16[1024,256]{1,0:T(8,128)(2,1)S(1)}, u32[]{:S(2)}, u32[]{:S(2)}) collective-permute-start(bf16[1024,256]{1,0:T(8,128)(2,1)} %get-tuple-element.29), channel_id=1, source_target_pairs={{0,6},{2,4},{4,2},{6,0},{1,7},{3,5},{5,3},{7,1},{8,14},{10,12},{12... | collective-permute-start | bytes 1572872 | tf_op jit(solution)/shard_map/ppermute | solution.py:274
  69.7 20.6 %collective-permute-start.3 = (f32[4,1,256]{2,1,0:T(1,128)S(1)}, f32[4,1,256]{2,1,0:T(1,128)S(1)}, u32[]{:S(2)}, u32[]{:S(2)}) collective-permute-start(f32[4,1,256]{2,1,0:T(1,128)S(1)} %get-tuple-element.30.refs_4_), channel_id=1, source_target_pairs={{0,2},{2,0},{4,6},{6,4},{1,3},{3,1},{5,7},{7,5},{8,10},{10,8},{12,... | collective-permute-start | bytes 12296 | tf_op jit(solution)/shard_map/ppermute | solution.py:274
  70.4 20.7 %collective-permute-start.4 = (f32[4,1,256]{2,1,0:T(1,128)S(1)}, f32[4,1,256]{2,1,0:T(1,128)S(1)}, u32[]{:S(2)}, u32[]{:S(2)}) collective-permute-start(f32[4,1,256]{2,1,0:T(1,128)S(1)} %get-tuple-element.30.refs_4_), channel_id=1, source_target_pairs={{0,4},{2,6},{4,0},{6,2},{1,5},{3,7},{5,1},{7,3},{8,12},{10,14},{12... | collective-permute-start | bytes 12296 | tf_op jit(solution)/shard_map/ppermute | solution.py:274
  114.1 14.9 %collective-permute-start.14 = (bf16[1024,256]{1,0:T(8,128)(2,1)S(1)}, bf16[1024,256]{1,0:T(8,128)(2,1)S(1)}, u32[]{:S(2)}, u32[]{:S(2)}) collective-permute-start(bf16[1024,256]{1,0:T(8,128)(2,1)S(1)} %hidden.2.refs_0_), channel_id=1, source_target_pairs={{0,2},{2,0},{4,6},{6,4},{1,3},{3,1},{5,7},{7,5},{8,10},{10,8},{12,... | collective-permute-start | bytes 1572872 | tf_op jit(solution)/shard_map/ppermute | solution.py:274
  115.4 20.1 %collective-permute-start.15 = (bf16[1024,256]{1,0:T(8,128)(2,1)S(1)}, bf16[1024,256]{1,0:T(8,128)(2,1)S(1)}, u32[]{:S(2)}, u32[]{:S(2)}) collective-permute-start(bf16[1024,256]{1,0:T(8,128)(2,1)S(1)} %hidden.2.refs_0_), channel_id=1, source_target_pairs={{0,4},{2,6},{4,0},{6,2},{1,5},{3,7},{5,1},{7,3},{8,12},{10,14},{12... | collective-permute-start | bytes 1572872 | tf_op jit(solution)/shard_map/ppermute | solution.py:274
  116.3 20.1 %collective-permute-start.16 = (bf16[1024,256]{1,0:T(8,128)(2,1)S(1)}, bf16[1024,256]{1,0:T(8,128)(2,1)S(1)}, u32[]{:S(2)}, u32[]{:S(2)}) collective-permute-start(bf16[1024,256]{1,0:T(8,128)(2,1)S(1)} %hidden.2.refs_0_), channel_id=1, source_target_pairs={{0,6},{2,4},{4,2},{6,0},{1,7},{3,5},{5,3},{7,1},{8,14},{10,12},{12... | collective-permute-start | bytes 1572872 | tf_op jit(solution)/shard_map/ppermute | solution.py:274
  157.8 29.4 %collective-permute-start.18 = (bf16[1024,256]{1,0:T(8,128)(2,1)S(1)}, bf16[1024,256]{1,0:T(8,128)(2,1)S(1)}, u32[]{:S(2)}, u32[]{:S(2)}) collective-permute-start(bf16[1024,256]{1,0:T(8,128)(2,1)S(1)} %get-tuple-element.38), channel_id=1, source_target_pairs={{0,2},{2,0},{4,6},{6,4},{1,3},{3,1},{5,7},{7,5},{8,10},{10,8},{12,... | collective-permute-start | bytes 1572872 | tf_op jit(solution)/shard_map/ppermute | solution.py:274
  159.3 27.9 %collective-permute-start.19 = (bf16[1024,256]{1,0:T(8,128)(2,1)S(1)}, bf16[1024,256]{1,0:T(8,128)(2,1)S(1)}, u32[]{:S(2)}, u32[]{:S(2)}) collective-permute-start(bf16[1024,256]{1,0:T(8,128)(2,1)S(1)} %get-tuple-element.39), channel_id=1, source_target_pairs={{0,4},{2,6},{4,0},{6,2},{1,5},{3,7},{5,1},{7,3},{8,12},{10,14},{12... | collective-permute-start | bytes 1572872 | tf_op jit(solution)/shard_map/ppermute | solution.py:274
  160.8 26.4 %collective-permute-start.20 = (bf16[1024,256]{1,0:T(8,128)(2,1)S(1)}, bf16[1024,256]{1,0:T(8,128)(2,1)S(1)}, u32[]{:S(2)}, u32[]{:S(2)}) collective-permute-start(bf16[1024,256]{1,0:T(8,128)(2,1)S(1)} %get-tuple-element.40), channel_id=1, source_target_pairs={{0,6},{2,4},{4,2},{6,0},{1,7},{3,5},{5,3},{7,1},{8,14},{10,12},{12... | collective-permute-start | bytes 1572872 | tf_op jit(solution)/shard_map/ppermute | solution.py:274
  161.3 21.4 %collective-permute-start.21 = (f32[4,1,256]{2,1,0:T(1,128)S(1)}, f32[4,1,256]{2,1,0:T(1,128)S(1)}, u32[]{:S(2)}, u32[]{:S(2)}) collective-permute-start(f32[4,1,256]{2,1,0:T(1,128)S(1)} %get-tuple-element.41.refs_4_), channel_id=1, source_target_pairs={{0,2},{2,0},{4,6},{6,4},{1,3},{3,1},{5,7},{7,5},{8,10},{10,8},{12,... | collective-permute-start | bytes 12296 | tf_op jit(solution)/shard_map/ppermute | solution.py:274
  162.8 22.2 %collective-permute-start.22 = (f32[4,1,256]{2,1,0:T(1,128)S(1)}, f32[4,1,256]{2,1,0:T(1,128)S(1)}, u32[]{:S(2)}, u32[]{:S(2)}) collective-permute-start(f32[4,1,256]{2,1,0:T(1,128)S(1)} %get-tuple-element.41.refs_4_), channel_id=1, source_target_pairs={{0,4},{2,6},{4,0},{6,2},{1,5},{3,7},{5,1},{7,3},{8,12},{10,14},{12... | collective-permute-start | bytes 12296 | tf_op jit(solution)/shard_map/ppermute | solution.py:274
  207.6 21.2 %collective-permute-start.29 = (bf16[1024,256]{1,0:T(8,128)(2,1)S(1)}, bf16[1024,256]{1,0:T(8,128)(2,1)S(1)}, u32[]{:S(2)}, u32[]{:S(2)}) collective-permute-start(bf16[1024,256]{1,0:T(8,128)(2,1)S(1)} %hidden.3.refs_0_), channel_id=1, source_target_pairs={{0,4},{2,6},{4,0},{6,2},{1,5},{3,7},{5,1},{7,3},{8,12},{10,14},{12... | collective-permute-start | bytes 1572872 | tf_op jit(solution)/shard_map/ppermute | solution.py:274
  209.0 19.8 %collective-permute-start.30 = (bf16[1024,256]{1,0:T(8,128)(2,1)S(1)}, bf16[1024,256]{1,0:T(8,128)(2,1)S(1)}, u32[]{:S(2)}, u32[]{:S(2)}) collective-permute-start(bf16[1024,256]{1,0:T(8,128)(2,1)S(1)} %hidden.3.refs_0_), channel_id=1, source_target_pairs={{0,6},{2,4},{4,2},{6,0},{1,7},{3,5},{5,3},{7,1},{8,14},{10,12},{12... | collective-permute-start | bytes 1572872 | tf_op jit(solution)/shard_map/ppermute | solution.py:274
  (32 other events, 169.1 us)
Sparse Core Ops, SparseCore 0:
  9.8 48.3 all-gather.8
  59.8 44.4 all-gather.10
  105.9 44.5 all-gather.12
  151.9 44.4 all-gather.14
